TPU v7x, 32 devices: a whole 2x2x4 slice. The times are simulated.
32 devices in a mesh: sp: 4 (over z), dp: 8 (over y, x, core).
Axes of the slice: x: 2, y: 2, z: 4, core: 2. Of those that a mesh axis runs over, the one named last changes fastest.
Arguments:
- normed: bfloat16 [8, 1024, 512], P('dp', None, 'sp'), may hold values from -6 to 6
- branch_in: bfloat16 [8, 1024, 512], P('dp', 'sp'), may hold values from -12 to 12
- gate_pre: bfloat16 [8, 1024, 512], P('dp', 'sp'), may hold values from -6 to 6
- cotangent: bfloat16 [8, 1024, 512], P('dp', None, 'sp'), may hold values from -6 to 6
- decay_shift: float32 [8, 16, 512], P('dp', 'sp'), may hold values from -1.2 to -0.000390625
- conv_weight: float32 [4, 1024], P(None, 'sp'), may hold values from -3 to 3
- recur_weight: float32 [16, 64, 64], P('sp'), may hold values from -0.75 to 0.75
- input_weight: float32 [16, 64, 64], P('sp'), may hold values from -0.75 to 0.75
- decay_param: float32 [1024], P('sp')
- branch_proj: bfloat16 [1024, 1024], P('dp'), may hold values from -0.1875 to 0.1875
Outputs:
- grad_normed: bfloat16 [8, 1024, 512], P('dp', None, 'sp')
- grad_gate: bfloat16 [8, 1024, 512], P('dp', 'sp')
- grad_proj: float32 [1024, 1024], P('dp', 'sp')
- grad_conv: float32 [4, 1024], P(None, 'sp')
- grad_recur: float32 [16, 64, 64], P('sp')
- grad_input: float32 [16, 64, 64], P('sp')
- grad_decay: float32 [1024], P('sp')
All inputs are finite; a program needn't handle non-finite values.
Results may differ from a plain program's by a relative error of at most 0.019.
Values may be sent and summed in bfloat16 or wider, within the bound.
A program may use at most 64 MiB of HBM per device.

v0:
```python
import math
import jax
import jax.numpy as jnp
from jax import lax
from jax.sharding import PartitionSpec as P

BLOCK_W = 64
CONV = 4
gate_const = 8.0
highest = lax.Precision.HIGHEST
far_below = -1e30


def block_states(log_decay, pushed):
    channels, length = pushed.shape
    span_len = math.gcd(length, 128)
    count = length // span_len
    logs = log_decay.reshape(channels, count, span_len).transpose(1, 0, 2)
    inputs = pushed.reshape(channels, count, span_len).transpose(1, 0, 2)
    places = jnp.arange(span_len)
    lower = places[:, None] >= places[None, :]

    @jax.checkpoint
    def advance(carry, items):
        block_logs, block_inputs = items
        running = jnp.cumsum(block_logs, axis=1)
        spread = running[:, :, None] - running[:, None, :]
        weights = jnp.exp(jnp.where(lower[None], spread, far_below))
        inner = jnp.einsum("cts,cs->ct", weights, block_inputs, precision=highest)
        states = inner + jnp.exp(running) * carry[:, None]
        return (states[:, -1], states)

    start = jnp.zeros((channels,), jnp.float32)
    _, blocks = lax.scan(advance, start, (logs, inputs))
    return blocks.transpose(1, 0, 2).reshape(channels, length)


def mixer(branch, gate, shift, conv_weight, recur_weight, input_weight, decay_param):
    channels, length = branch.shape
    padded = jnp.pad(branch, ((0, 0), (CONV - 1, 0)))
    convolved = conv_weight[0][:, None] * padded[:, 0:length]
    for offset in range(1, CONV):
        convolved = convolved + conv_weight[offset][:, None] * padded[:, offset : offset + length]
    groups = channels // BLOCK_W
    grouped = convolved.reshape(groups, BLOCK_W, length)
    recur_gate = jax.nn.sigmoid(
        jnp.einsum("gil,gij->gjl", grouped, recur_weight, precision=highest).reshape(
            channels, length
        )
    )
    input_gate = jax.nn.sigmoid(
        jnp.einsum("gil,gij->gjl", grouped, input_weight, precision=highest).reshape(
            channels, length
        )
    )
    log_decay = -gate_const * recur_gate * jax.nn.softplus(-decay_param)[:, None] + jnp.repeat(
        shift, BLOCK_W, axis=0
    )
    pushed = jnp.sqrt(-jnp.expm1(2.0 * log_decay)) * input_gate * convolved
    states = block_states(log_decay, pushed)
    return states * jax.nn.gelu(gate)


def mixer_grads(
    branch, gate, shift, upstream, conv_weight, recur_weight, input_weight, decay_param
):

    def local(branch_f, gate_f, conv_f, recur_f, input_f, decay_f):
        return mixer(branch_f, gate_f, shift, conv_f, recur_f, input_f, decay_f)

    _, pullback = jax.vjp(
        local,
        branch.astype(jnp.float32),
        gate.astype(jnp.float32),
        conv_weight,
        recur_weight,
        input_weight,
        decay_param,
    )
    return pullback(upstream.astype(jnp.float32))


def body(
    normed,
    branch_in,
    gate_pre,
    cotangent,
    decay_shift,
    conv_weight,
    recur_weight,
    input_weight,
    decay_param,
    branch_proj,
):
    heads_cot = lax.all_to_all(cotangent, "sp", split_axis=1, concat_axis=2, tiled=True)
    grad_branch, grad_gate, grad_conv, grad_recur, grad_input, grad_decay = mixer_grads(
        branch_in[0],
        gate_pre[0],
        decay_shift[0],
        heads_cot[0],
        conv_weight,
        recur_weight,
        input_weight,
        decay_param,
    )
    small_sums = (
        lax.psum(grad_conv.astype(jnp.bfloat16), "dp").astype(jnp.float32),
        lax.psum(grad_recur.astype(jnp.bfloat16), "dp").astype(jnp.float32),
        lax.psum(grad_input.astype(jnp.bfloat16), "dp").astype(jnp.float32),
        lax.psum(grad_decay.astype(jnp.bfloat16), "dp").astype(jnp.float32),
    )
    branch_rounded = grad_branch.astype(jnp.bfloat16)[None]
    token_grad = lax.all_to_all(branch_rounded, "sp", split_axis=2, concat_axis=1, tiled=True)[0]
    grad_normed = jnp.dot(
        lax.all_gather(branch_proj, "dp", axis=0, tiled=True),
        token_grad,
        preferred_element_type=jnp.float32,
    ).astype(jnp.bfloat16)[None]
    partial_sum = lax.dot_general(
        normed[0], token_grad, (((1,), (1,)), ((), ())), preferred_element_type=jnp.float32
    )
    received = lax.all_to_all(
        partial_sum[None].astype(jnp.bfloat16), "dp", split_axis=1, concat_axis=0, tiled=True
    ).astype(jnp.float32)
    row_block = jnp.sum(received, axis=0)
    seq_count = lax.axis_size("sp")
    rows_here = row_block.shape[0]
    width_share = row_block.shape[1] // seq_count
    stacked = (
        row_block.reshape(rows_here, seq_count, width_share)
        .transpose(1, 0, 2)
        .reshape(seq_count * rows_here, width_share)
    )
    grad_proj = lax.psum_scatter(stacked, "sp", scatter_dimension=0, tiled=True)
    return (
        grad_normed,
        grad_gate.astype(jnp.bfloat16)[None],
        grad_proj,
        small_sums[0],
        small_sums[1],
        small_sums[2],
        small_sums[3],
    )


def solution(mesh):
    return jax.shard_map(
        body,
        mesh=mesh,
        in_specs=(
            P("dp", None, "sp"),
            P("dp", "sp", None),
            P("dp", "sp", None),
            P("dp", None, "sp"),
            P("dp", "sp", None),
            P(None, "sp"),
            P("sp", None, None),
            P("sp", None, None),
            P("sp"),
            P("dp", None),
        ),
        out_specs=(
            P("dp", None, "sp"),
            P("dp", "sp", None),
            P("dp", "sp"),
            P(None, "sp"),
            P("sp", None, None),
            P("sp", None, None),
            P("sp"),
        ),
        check_vma=False,
    )
```

profile of v0, /device:TPU:0, one launch (start us, length us, event | category | flops | bytes accessed | tf_op | source)
XLA Modules:
  0.0 484.7 jit_solution(2969427192037989468)
XLA Ops:
  8.0 1.4 copy.271
  10.0 2.2 reduce.1
  12.9 6.3 %all-to-all-start = ((bf16[4,2,16384]{2,1,0:T(2,128)(2,1)}), bf16[4,2,16384]{2,1,0:T(2,128)(2,1)}, u32[]{:S(2)}, u32[]{:S(2)}) async-start(bf16[4,2,16384]{2,1,0:T(2,128)(2,1)} %reshape.215), calls=%async_computation | async-start | bytes 524288 | tf_op jit(solution)/shard_map/all_to_all | solution.py:95
  30.4 131.4 %while.35 = (s32[]{:T(128)}, f32[256]{0:T(256)S(1)}, f32[4,256,128]{1,2,0:T(8,128)}, f32[4,256]{1,0:T(4,128)}, f32[4,256,128]{1,2,0:T(8,128)S(1)}, /*index=5*/f3...) while((s32[]{:T(128)}, f32[256]{0:T(256)S(1)}, ...), condition=%wide.region_2.3_spmd.clone, body=%wide.region_0.2_spmd.clone.sunk | while | flops 62947328 | bytes 2249857 | solution.py:34
  30.7 1.3 dynamic_update_slice.42
  32.3 27.3 %fusion.93 = f32[256,1,128]{2,1,0:T(1,128)S(1)} fusion(f32[256,128,1]{1,2,0:T(1,128)S(1)} %bitcast.252, f32[256,128]{1,0:T(8,128)S(1)} %copy.280, pred[128,128]{1,0:T(8,128)(4,1)S(1)} %get-tuple-element.650), kind=kOutput, calls=%fused_computation.2.clone.1 | convolution fusion | flops 58720256 | bytes 409600 | tf_op jit(solution)/shard_map/jvp()/while/body/eval_jaxpr/cts,cs->ct/dot_general | solution.py:29
  60.4 1.3 dynamic_update_slice.42
  62.0 27.3 %fusion.93 = f32[256,1,128]{2,1,0:T(1,128)S(1)} fusion(f32[256,128,1]{1,2,0:T(1,128)S(1)} %bitcast.252, f32[256,128]{1,0:T(8,128)S(1)} %copy.280, pred[128,128]{1,0:T(8,128)(4,1)S(1)} %get-tuple-element.650), kind=kOutput, calls=%fused_computation.2.clone.1 | convolution fusion | flops 58720256 | bytes 409600 | tf_op jit(solution)/shard_map/jvp()/while/body/eval_jaxpr/cts,cs->ct/dot_general | solution.py:29
  91.7 27.3 %fusion.93 = f32[256,1,128]{2,1,0:T(1,128)S(1)} fusion(f32[256,128,1]{1,2,0:T(1,128)S(1)} %bitcast.252, f32[256,128]{1,0:T(8,128)S(1)} %copy.280, pred[128,128]{1,0:T(8,128)(4,1)S(1)} %get-tuple-element.650), kind=kOutput, calls=%fused_computation.2.clone.1 | convolution fusion | flops 58720256 | bytes 409600 | tf_op jit(solution)/shard_map/jvp()/while/body/eval_jaxpr/cts,cs->ct/dot_general | solution.py:29
  121.4 27.3 %fusion.93 = f32[256,1,128]{2,1,0:T(1,128)S(1)} fusion(f32[256,128,1]{1,2,0:T(1,128)S(1)} %bitcast.252, f32[256,128]{1,0:T(8,128)S(1)} %copy.280, pred[128,128]{1,0:T(8,128)(4,1)S(1)} %get-tuple-element.650), kind=kOutput, calls=%fused_computation.2.clone.1 | convolution fusion | flops 58720256 | bytes 409600 | tf_op jit(solution)/shard_map/jvp()/while/body/eval_jaxpr/cts,cs->ct/dot_general | solution.py:29
  164.6 1.9 reshape.216
  168.2 2.0 fusion.29
  172.6 173.6 %while.36 = (s32[]{:T(128)}, f32[256]{0:T(256)}, f32[4,256,128]{1,2,0:T(8,128)}, f32[4,256,128]{2,1,0:T(8,128)}, f32[4,256]{1,0:T(4,128)}, /*index=5*/f32[4,256,...) while((s32[]{:T(128)}, f32[256]{0:T(256)}, ...), condition=%wide.region_9.10_spmd.clone, body=%wide.region_3.9_spmd.clone.sunk | while | flops 96616192 | bytes 5561497 | solution.py:34
  176.6 16.0 %fusion.96 = f32[256,1,128]{2,1,0:T(1,128)} fusion(f32[256,128,1]{1,2,0:T(1,128)S(1)} %copy.287, f32[256,128]{1,0:T(8,128)S(1)} %copy.283, pred[128,128]{1,0:T(8,128)(4,1)S(1)} %iota_compare_fusion.3), kind=kOutput, calls=%fused_computation.17.clone.1 | convolution fusion | flops 58720256 | bytes 409600 | tf_op jit(solution)/shard_map/transpose(jvp())/while/body/eval_jaxpr/checkpoint/cts,cs->ct/dot_general | solution.py:29
  193.3 16.3 %fusion.95 = (f32[256,128]{1,0:T(8,128)}, f32[256,128]{1,0:T(8,128)S(1)}) fusion(f32[256,128]{1,0:T(8,128)S(1)} %copy.283, f32[256,128]{1,0:T(8,128)S(1)} %dynamic-slice_bitcast_fusion.8, f32[256,128]{1,0:T(8,128)} %copy.284, pred[128,128]{1,0:T(8,128)(4,1)S(1)} %iota_compare_fusion.3), kind=kLoop, calls=%fused_computation.19.clone.1 | loop fusion | flops 29294592 | bytes 671744 | tf_op jit(solution)/shard_map/transpose(jvp())/while/body/eval_jaxpr/checkpoint/reduce_sum | solution.py:27
  211.5 2.2 reduce_window_sum.48
  214.3 1.6 bitcast_dynamic-update-slice_fusion.5
  220.0 16.0 %fusion.96 = f32[256,1,128]{2,1,0:T(1,128)} fusion(f32[256,128,1]{1,2,0:T(1,128)S(1)} %copy.287, f32[256,128]{1,0:T(8,128)S(1)} %copy.283, pred[128,128]{1,0:T(8,128)(4,1)S(1)} %iota_compare_fusion.3), kind=kOutput, calls=%fused_computation.17.clone.1 | convolution fusion | flops 58720256 | bytes 409600 | tf_op jit(solution)/shard_map/transpose(jvp())/while/body/eval_jaxpr/checkpoint/cts,cs->ct/dot_general | solution.py:29
  236.7 16.3 %fusion.95 = (f32[256,128]{1,0:T(8,128)}, f32[256,128]{1,0:T(8,128)S(1)}) fusion(f32[256,128]{1,0:T(8,128)S(1)} %copy.283, f32[256,128]{1,0:T(8,128)S(1)} %dynamic-slice_bitcast_fusion.8, f32[256,128]{1,0:T(8,128)} %copy.284, pred[128,128]{1,0:T(8,128)(4,1)S(1)} %iota_compare_fusion.3), kind=kLoop, calls=%fused_computation.19.clone.1 | loop fusion | flops 29294592 | bytes 671744 | tf_op jit(solution)/shard_map/transpose(jvp())/while/body/eval_jaxpr/checkpoint/reduce_sum | solution.py:27
  254.8 2.2 reduce_window_sum.48
  257.7 1.6 bitcast_dynamic-update-slice_fusion.5
  263.3 16.0 %fusion.96 = f32[256,1,128]{2,1,0:T(1,128)} fusion(f32[256,128,1]{1,2,0:T(1,128)S(1)} %copy.287, f32[256,128]{1,0:T(8,128)S(1)} %copy.283, pred[128,128]{1,0:T(8,128)(4,1)S(1)} %iota_compare_fusion.3), kind=kOutput, calls=%fused_computation.17.clone.1 | convolution fusion | flops 58720256 | bytes 409600 | tf_op jit(solution)/shard_map/transpose(jvp())/while/body/eval_jaxpr/checkpoint/cts,cs->ct/dot_general | solution.py:29
  280.0 16.3 %fusion.95 = (f32[256,128]{1,0:T(8,128)}, f32[256,128]{1,0:T(8,128)S(1)}) fusion(f32[256,128]{1,0:T(8,128)S(1)} %copy.283, f32[256,128]{1,0:T(8,128)S(1)} %dynamic-slice_bitcast_fusion.8, f32[256,128]{1,0:T(8,128)} %copy.284, pred[128,128]{1,0:T(8,128)(4,1)S(1)} %iota_compare_fusion.3), kind=kLoop, calls=%fused_computation.19.clone.1 | loop fusion | flops 29294592 | bytes 671744 | tf_op jit(solution)/shard_map/transpose(jvp())/while/body/eval_jaxpr/checkpoint/reduce_sum | solution.py:27
  298.2 2.2 reduce_window_sum.48
  301.0 1.6 bitcast_dynamic-update-slice_fusion.5
  306.6 16.0 %fusion.96 = f32[256,1,128]{2,1,0:T(1,128)} fusion(f32[256,128,1]{1,2,0:T(1,128)S(1)} %copy.287, f32[256,128]{1,0:T(8,128)S(1)} %copy.283, pred[128,128]{1,0:T(8,128)(4,1)S(1)} %iota_compare_fusion.3), kind=kOutput, calls=%fused_computation.17.clone.1 | convolution fusion | flops 58720256 | bytes 409600 | tf_op jit(solution)/shard_map/transpose(jvp())/while/body/eval_jaxpr/checkpoint/cts,cs->ct/dot_general | solution.py:29
  323.4 16.3 %fusion.95 = (f32[256,128]{1,0:T(8,128)}, f32[256,128]{1,0:T(8,128)S(1)}) fusion(f32[256,128]{1,0:T(8,128)S(1)} %copy.283, f32[256,128]{1,0:T(8,128)S(1)} %dynamic-slice_bitcast_fusion.8, f32[256,128]{1,0:T(8,128)} %copy.284, pred[128,128]{1,0:T(8,128)(4,1)S(1)} %iota_compare_fusion.3), kind=kLoop, calls=%fused_computation.19.clone.1 | loop fusion | flops 29294592 | bytes 671744 | tf_op jit(solution)/shard_map/transpose(jvp())/while/body/eval_jaxpr/checkpoint/reduce_sum | solution.py:27
  341.5 2.2 reduce_window_sum.48
  344.4 1.6 bitcast_dynamic-update-slice_fusion.5
  346.2 2.1 copy.250
  348.3 2.1 copy.231
  351.7 2.9 fusion.52
  355.8 1.4 fusion.67
  358.3 2.1 reshape.202
  363.4 2.3 fusion.48
  369.3 2.2 reduce.2
  371.6 13.2 %all_to_all.33 = bf16[4,2,16384]{2,1,0:T(2,128)(2,1)S(1)} all-to-all(bf16[4,2,16384]{2,1,0:T(2,128)(2,1)S(1)} %reshape.217), channel_id=1, replica_groups=mesh['sp'=4,'dp'=8] {'sp'}, dimensions={0} | all-to-all | bytes 524288 | tf_op jit(solution)/shard_map/all_to_all | solution.py:113
  386.0 7.7 %copy.238 = bf16[1,1024,1024]{2,0,1:T(2,128)(2,1)} copy(bf16[1,1024,1024]{1,2,0:T(8,128)(2,1)S(1)} %convert_bitcast_fusion) | data formatting | bytes 4194304 | tf_op jit(solution)/shard_map/convert_element_type | solution.py:123
  393.8 12.7 %reduce.3 = bf16[1024,1024]{1,0:T(8,128)(2,1)S(1)} reduce(bf16[1024,1,1024]{2,1,0:T(2,128)(2,1)} %bitcast.238, bf16[]{:T(256)} %broadcast.172), dimensions={1}, to_apply=%bitcast.175.reduce_sub_computation | reduce | bytes 4194306
  406.5 3.8 reshape.219
  410.3 33.4 %all_to_all.34 = bf16[8,2,65536]{2,1,0:T(2,128)(2,1)S(1)} all-to-all(bf16[8,2,65536]{2,1,0:T(2,128)(2,1)} %reshape.219), channel_id=1, replica_groups=mesh['sp'=4,'dp'=8] {'dp'}, dimensions={0} | all-to-all | bytes 4194304 | tf_op jit(solution)/shard_map/all_to_all | solution.py:122
  443.7 4.4 reshape.220
  448.1 5.2 %copy.254 = f32[1,1024,1024]{2,1,0:T(8,128)} copy(bf16[1,1024,1024]{2,0,1:T(2,128)(2,1)} %bitcast.240) | data formatting | bytes 6291456
  453.3 2.7 reduce_sum.117
  461.2 1.5 convert_element_type.128
  462.7 1.5 convert_element_type.130
  464.2 2.4 fusion.27
  467.4 9.4 %reduce-scatter.2.cloned.1.call-done = f32[128,256]{1,0:T(8,128)} async-done(((f32[512,256]{1,0:T(8,128)}), f32[128,256]{1,0:T(8,128)}) %reduce-scatter.2.cloned.1.call-update) | async-done | bytes 131088 | tf_op jit(solution)/shard_map/reduce_scatter | solution.py:134
  (211 shorter events, 72.3 us)
Async XLA Ops:
  8.0 377.3 %copy-start = (bf16[1,1024,128]{2,1,0:T(8,128)(2,1)S(1)}, bf16[1,1024,128]{2,1,0:T(8,128)(2,1)}, u32[]{:S(2)}) copy-start(bf16[1,1024,128]{2,1,0:T(8,128)(2,1)} %param.14) | copy-start | bytes 786436
  8.0 15.1 %copy-start.13 = (f32[4,64,64]{2,1,0:T(8,128)S(1)}, f32[4,64,64]{2,1,0:T(8,128)}, u32[]{:S(2)}) copy-start(f32[4,64,64]{2,1,0:T(8,128)} %param.20) | copy-start | bytes 196612
  8.0 15.9 %copy-start.11 = (f32[4,64,64]{2,1,0:T(8,128)S(1)}, f32[4,64,64]{2,1,0:T(8,128)}, u32[]{:S(2)}) copy-start(f32[4,64,64]{2,1,0:T(8,128)} %param.21) | copy-start | bytes 196612
  9.4 15.2 %copy-start.9 = (f32[1,4,512]{2,1,0:T(4,128)S(1)}, f32[1,4,512]{2,1,0:T(4,128)}, u32[]{:S(2)}) copy-start(f32[1,4,512]{2,1,0:T(4,128)} %param.18) | copy-start | bytes 24580
  12.9 151.6 %all-to-all-start = ((bf16[4,2,16384]{2,1,0:T(2,128)(2,1)}), bf16[4,2,16384]{2,1,0:T(2,128)(2,1)}, u32[]{:S(2)}, u32[]{:S(2)}) async-start(bf16[4,2,16384]{2,1,0:T(2,128)(2,1)} %reshape.215), calls=%async_computation | async-start | bytes 524288 | tf_op jit(solution)/shard_map/all_to_all | solution.py:95
  19.3 439.4 %all-reduce.13.cloned.1.call-start = ((), (), s32[]{:S(2)}) async-start(), calls=%async_computation.6 | async-start | bytes 267264 | tf_op jit(solution)/shard_map/psum | solution.py:107
  20.6 141.3 %copy-start.14 = (f32[256]{0:T(256)}, f32[256]{0:T(256)S(1)}, u32[]{:S(2)}) copy-start(f32[256]{0:T(256)S(1)} %get-tuple-element.495) | copy-start | bytes 3076
  21.4 4.1 copy-start.16
  21.4 4.1 copy-start.18
  21.4 4.1 copy-start.20
  21.4 4.1 copy-start.22
  23.1 0.8 copy-start.1
  163.6 8.9 %copy-start.6 = (bf16[1,256,512]{1,2,0:T(8,128)(2,1)}, bf16[1,256,512]{1,2,0:T(8,128)(2,1)S(1)}, u32[]{:S(2)}) copy-start(bf16[1,256,512]{1,2,0:T(8,128)(2,1)S(1)} %copy.222) | copy-start | bytes 786436
  167.5 0.7 copy-start.4
  346.1 8.4 %copy-start.2 = (f32[256,512]{1,0:T(8,128)S(1)}, f32[256,512]{1,0:T(8,128)}, u32[]{:S(2)}) copy-start(f32[256,512]{1,0:T(8,128)} %copy-done.1) | copy-start | bytes 1572868
  348.3 8.9 %copy-start.3 = (f32[4,256,128]{2,1,0:T(8,128)S(1)}, f32[4,256,128]{2,1,0:T(8,128)}, u32[]{:S(2)}) copy-start(f32[4,256,128]{2,1,0:T(8,128)} %get-tuple-element.258) | copy-start | bytes 1572868
  351.6 4.2 copy-start.12
  351.6 8.8 %copy-start.24 = (f32[256]{0:T(256)S(1)}, f32[256]{0:T(256)}, u32[]{:S(2)}) copy-start(f32[256]{0:T(256)} %get-tuple-element.496) | copy-start | bytes 3076
  351.7 8.7 %copy-start.26 = (f32[256]{0:T(256)S(1)}, f32[256]{0:T(256)}, u32[]{:S(2)}) copy-start(f32[256]{0:T(256)} %param.22) | copy-start | bytes 3076
  354.5 8.9 %copy-start.10 = (f32[1,4,512]{2,1,0:T(4,128)S(1)}, f32[1,4,512]{2,1,0:T(4,128)}, u32[]{:S(2)}) copy-start(f32[1,4,512]{2,1,0:T(4,128)} %param.18) | copy-start | bytes 24580
  354.5 8.9 %copy-start.25 = (f32[4,64]{1,0:T(4,128)S(1)}, f32[4,64]{1,0:T(4,128)}, u32[]{:S(2)}) copy-start(f32[4,64]{1,0:T(4,128)} %mul.371) | copy-start | bytes 3076
  357.2 8.6 %copy-start.15 = (f32[256]{0:T(256)S(1)}, f32[256]{0:T(256)}, u32[]{:S(2)}) copy-start(f32[256]{0:T(256)} %copy-done.14) | copy-start | bytes 3076
  362.1 6.0 %copy-start.17 = (f32[1,256]{1,0:T(1,128)S(1)}, f32[1,256]{1,0:T(1,128)}, u32[]{:S(2)}) copy-start(f32[1,256]{1,0:T(1,128)} %copy-done.16) | copy-start | bytes 3076
  362.1 6.0 %copy-start.19 = (f32[1,256]{1,0:T(1,128)S(1)}, f32[1,256]{1,0:T(1,128)}, u32[]{:S(2)}) copy-start(f32[1,256]{1,0:T(1,128)} %copy-done.18) | copy-start | bytes 3076
  362.2 6.0 %copy-start.21 = (f32[1,256]{1,0:T(1,128)S(1)}, f32[1,256]{1,0:T(1,128)}, u32[]{:S(2)}) copy-start(f32[1,256]{1,0:T(1,128)} %copy-done.20) | copy-start | bytes 3076
  362.2 6.0 %copy-start.23 = (f32[1,256]{1,0:T(1,128)S(1)}, f32[1,256]{1,0:T(1,128)}, u32[]{:S(2)}) copy-start(f32[1,256]{1,0:T(1,128)} %copy-done.22) | copy-start | bytes 3076
  367.4 96.8 %all-gather.2.cloned.1.call-start = ((), (), s32[]{:S(2)}) async-start(), calls=%async_computation.4 | async-start | bytes 2359296 | tf_op jit(solution)/shard_map/all_gather | solution.py:115
  368.1 108.8 %reduce-scatter.2.cloned.1.call-start = ((), (), s32[]{:S(2)}) async-start(), calls=%async_computation.5 | async-start | bytes 655360 | tf_op jit(solution)/shard_map/reduce_scatter | solution.py:134
  453.3 4.0 copy-start.5
  453.3 4.2 copy-start.7
  453.3 4.2 copy-start.8
Sparse Core Ops, SparseCore 0:
  367.5 53.7 all-reduce.12
  423.2 32.6 all-gather.1
Sparse Core Ops, SparseCore 1:
  457.3 19.5 reduce-scatter.1
where the time goes:
time: 492 us; the launch traced here: 485 us
  matrix products  184 us (37%)
  other arithmetic  123 us (25%)
  local copies, waits for them, and re-layouts  85.1 us (17%)
  blocking collectives  46.6 us (9%)
  between operations  16.5 us (3%)
  loops' own time  13.2 us (3%)
  waiting for transfers between devices  10.1 us (2%)
  starting transfers between devices  6.43 us (1%)
    dot_general x8, matrix products, advance(): inner = jnp.einsum('cts,cs->ct', weights, block_inputs, precision=highest)  173 us
    reduce_sum x4, other arithmetic, advance(): spread = running[:, :, None] - running[:, None, :]  65.3 us
    all_to_all x1, blocking collectives, body(): lax.all_to_all(partial_sum[None].astype(jnp.bfloat16), 'dp', split_axis=1...  33.4 us
    unnamed x68, local copies, waits for them, and re-layouts  22.2 us
    unnamed x3, other arithmetic  17.1 us
    dynamic_update_slice x12, local copies, waits for them, and re-layouts, block_states(): _, blocks = lax.scan(advance, start, (logs, inputs))  14.2 us
    another operation x2, loops' own time, block_states(): _, blocks = lax.scan(advance, start, (logs, inputs))  13.2 us
    all_to_all x1, blocking collectives, body(): lax.all_to_all(branch_rounded, 'sp', split_axis=2, concat_axis=1, tiled=T...  13.2 us
  transfers between devices with their start and end apart: 4, of which 1 were waited for; matrix products, arithmetic and copies ran while one was open for 38% of the time, Pallas kernels for 0%

commit v1 on v0

--- a/solution.py
+++ b/solution.py
@@ -9,6 +9,13 @@
 gate_const = 8.0
 highest = lax.Precision.HIGHEST
 far_below = -1e30
+
+
+def stacked_exchange(value, axis, split, join):
+    size = lax.axis_size(axis)
+    parts = jnp.stack(jnp.split(value, size, axis=split), axis=0)
+    parts = lax.all_to_all(parts, axis, split_axis=0, concat_axis=0)
+    return jnp.concatenate(parts, axis=join)
 
 
 def block_states(log_decay, pushed):
@@ -119,9 +126,9 @@
     partial_sum = lax.dot_general(
         normed[0], token_grad, (((1,), (1,)), ((), ())), preferred_element_type=jnp.float32
     )
-    received = lax.all_to_all(
-        partial_sum[None].astype(jnp.bfloat16), "dp", split_axis=1, concat_axis=0, tiled=True
-    ).astype(jnp.float32)
+    received = stacked_exchange(partial_sum[None].astype(jnp.bfloat16), "dp", 1, 0).astype(
+        jnp.float32
+    )
     row_block = jnp.sum(received, axis=0)
     seq_count = lax.axis_size("sp")
     rows_here = row_block.shape[0]

time: 492 us -> 467 us (0.949)
  waiting for transfers between devices: 10.1 us -> 46.9 us
  local copies, waits for them, and re-layouts: 85.1 us -> 55.4 us
  other arithmetic: 123 us -> 106 us
  blocking collectives: 46.6 us -> 30.7 us
  starting transfers between devices: 6.43 us -> 11.5 us
    all_gather x1, waiting for transfers between devices: 0.01 us -> 25 us  [body(): lax.all_gather(branch_proj, 'dp', axis=0, tiled=True)]
    all_to_all x2 -> x1, blocking collectives: 46.6 us -> 30.7 us  [stacked_exchange(): parts = lax.all_to_all(parts, axis, split_axis=0, concat_axis=0)]
    psum x1, waiting for transfers between devices: 0.01 us -> 15.5 us  [body(): lax.psum(grad_conv.astype(jnp.bfloat16), 'dp').astype(jnp.float32)]
    unnamed x3 -> x2, other arithmetic: 17.1 us -> 4.36 us
    unnamed x68 -> x100, local copies, waits for them, and re-layouts: 22.2 us -> 10.1 us
    reduce_scatter x1, waiting for transfers between devices: 9.41 us -> 0.01 us  [body(): grad_proj = lax.psum_scatter(stacked, 'sp', scatter_dimension=0, tiled=True)]
    convert_element_type x1 -> x0, local copies, waits for them, and re-layouts: 7.74 us -> none  [body(): partial_sum[None].astype(jnp.bfloat16)]
    all_to_all x0 -> x1, waiting for transfers between devices: none -> 5.65 us  [body(): lax.all_to_all(branch_rounded, 'sp', split_axis=2, concat_axis=1, tiled=T...]
  transfers between devices with their start and end apart: 4 -> 5, of which waited for: 1 -> 3; matrix products, arithmetic and copies ran while one was open for 38% -> 31% of each run, Pallas kernels for 0% -> 0%
where the time goes in v1:
time: 467 us; the launch traced here: 460 us
  matrix products  180 us (39%)
  other arithmetic  106 us (23%)
  local copies, waits for them, and re-layouts  55.4 us (12%)
  waiting for transfers between devices  46.9 us (10%)
  blocking collectives  30.7 us (7%)
  between operations  16.6 us (4%)
  loops' own time  13.2 us (3%)
  starting transfers between devices  11.5 us (2%)
    dot_general x8, matrix products, advance(): inner = jnp.einsum('cts,cs->ct', weights, block_inputs, precision=highest)  170 us
    reduce_sum x4, other arithmetic, advance(): spread = running[:, :, None] - running[:, None, :]  65.3 us
    all_to_all x1, blocking collectives, stacked_exchange(): parts = lax.all_to_all(parts, axis, split_axis=0, concat_axis=0)  30.7 us
    all_gather x1, waiting for transfers between devices, body(): lax.all_gather(branch_proj, 'dp', axis=0, tiled=True)  25 us
    psum x1, waiting for transfers between devices, body(): lax.psum(grad_conv.astype(jnp.bfloat16), 'dp').astype(jnp.float32)  15.5 us
    another operation x16, other arithmetic, advance(): running = jnp.cumsum(block_logs, axis=1)  13.2 us
    another operation x2, loops' own time, block_states(): _, blocks = lax.scan(advance, start, (logs, inputs))  13.2 us
    dynamic_update_slice x12, local copies, waits for them, and re-layouts, block_states(): _, blocks = lax.scan(advance, start, (logs, inputs))  10.5 us
  transfers between devices with their start and end apart: 5, of which 3 were waited for; matrix products, arithmetic and copies ran while one was open for 31% of the time, Pallas kernels for 0%

profile of v1, /device:TPU:0, one launch (start us, length us, event | category | flops | bytes accessed | tf_op | source)
XLA Modules:
  0.0 460.2 jit_solution(629386554679617187)
XLA Ops:
  8.0 1.4 copy.231
  10.0 2.2 reduce.2
  13.0 6.3 %all-to-all-start = ((bf16[4,2,16384]{2,1,0:T(2,128)(2,1)}), bf16[4,2,16384]{2,1,0:T(2,128)(2,1)}, u32[]{:S(2)}, u32[]{:S(2)}) async-start(bf16[4,2,16384]{2,1,0:T(2,128)(2,1)} %reshape.211), calls=%async_computation | async-start | bytes 524288 | tf_op jit(solution)/shard_map/all_to_all | solution.py:102
  27.0 131.4 %while.35 = (s32[]{:T(128)}, f32[256]{0:T(256)S(1)}, f32[4,256,128]{1,2,0:T(8,128)}, f32[4,256]{1,0:T(4,128)}, f32[4,256,128]{1,2,0:T(8,128)S(1)}, /*index=5*/f3...) while((s32[]{:T(128)}, f32[256]{0:T(256)S(1)}, ...), condition=%wide.region_2.3_spmd.clone, body=%wide.region_0.2_spmd.clone.sunk | while | flops 62947328 | bytes 2250357 | solution.py:41
  27.5 27.3 %fusion.101 = f32[256,1,128]{2,1,0:T(1,128)S(1)} fusion(f32[256,128,1]{1,2,0:T(1,128)S(1)} %bitcast.277, f32[256,128]{1,0:T(8,128)S(1)} %copy.240, pred[128,128]{1,0:T(8,128)(4,1)S(1)} %get-tuple-element.628), kind=kOutput, calls=%fused_computation.2.clone.1 | convolution fusion | flops 58720256 | bytes 409600 | tf_op jit(solution)/shard_map/jvp()/while/body/eval_jaxpr/cts,cs->ct/dot_general | solution.py:36
  55.6 1.3 dynamic_update_slice.42
  57.2 27.3 %fusion.101 = f32[256,1,128]{2,1,0:T(1,128)S(1)} fusion(f32[256,128,1]{1,2,0:T(1,128)S(1)} %bitcast.277, f32[256,128]{1,0:T(8,128)S(1)} %copy.240, pred[128,128]{1,0:T(8,128)(4,1)S(1)} %get-tuple-element.628), kind=kOutput, calls=%fused_computation.2.clone.1 | convolution fusion | flops 58720256 | bytes 409600 | tf_op jit(solution)/shard_map/jvp()/while/body/eval_jaxpr/cts,cs->ct/dot_general | solution.py:36
  85.3 1.3 dynamic_update_slice.42
  86.9 27.3 %fusion.101 = f32[256,1,128]{2,1,0:T(1,128)S(1)} fusion(f32[256,128,1]{1,2,0:T(1,128)S(1)} %bitcast.277, f32[256,128]{1,0:T(8,128)S(1)} %copy.240, pred[128,128]{1,0:T(8,128)(4,1)S(1)} %get-tuple-element.628), kind=kOutput, calls=%fused_computation.2.clone.1 | convolution fusion | flops 58720256 | bytes 409600 | tf_op jit(solution)/shard_map/jvp()/while/body/eval_jaxpr/cts,cs->ct/dot_general | solution.py:36
  115.0 1.3 dynamic_update_slice.42
  116.6 27.3 %fusion.101 = f32[256,1,128]{2,1,0:T(1,128)S(1)} fusion(f32[256,128,1]{1,2,0:T(1,128)S(1)} %bitcast.277, f32[256,128]{1,0:T(8,128)S(1)} %copy.240, pred[128,128]{1,0:T(8,128)(4,1)S(1)} %get-tuple-element.628), kind=kOutput, calls=%fused_computation.2.clone.1 | convolution fusion | flops 58720256 | bytes 409600 | tf_op jit(solution)/shard_map/jvp()/while/body/eval_jaxpr/cts,cs->ct/dot_general | solution.py:36
  144.7 1.3 dynamic_update_slice.42
  161.1 1.9 reshape.212
  164.7 2.0 fusion.29
  169.1 167.3 %while.36 = (s32[]{:T(128)}, f32[256]{0:T(256)}, f32[4,256,128]{1,2,0:T(8,128)}, f32[4,256,128]{2,1,0:T(8,128)}, f32[4,256]{1,0:T(4,128)}, /*index=5*/f32[4,256,...) while((s32[]{:T(128)}, f32[256]{0:T(256)}, ...), condition=%wide.region_9.10_spmd.clone, body=%wide.region_3.9_spmd.clone.sunk | while | flops 96616192 | bytes 5561497 | solution.py:41
  170.1 1.3 constant_dynamic-slice_fusion.7
  173.1 15.3 %fusion.104 = f32[256,1,128]{2,1,0:T(1,128)S(1)} fusion(f32[256,128,1]{1,2,0:T(1,128)S(1)} %copy.247, f32[256,128]{1,0:T(8,128)S(1)} %copy.243, pred[128,128]{1,0:T(8,128)(4,1)S(1)} %iota_compare_fusion.3), kind=kOutput, calls=%fused_computation.17.clone.1 | convolution fusion | flops 58720256 | bytes 409600 | tf_op jit(solution)/shard_map/transpose(jvp())/while/body/eval_jaxpr/checkpoint/cts,cs->ct/dot_general | solution.py:36
  189.8 16.3 %fusion.103 = (f32[256,128]{1,0:T(8,128)}, f32[256,128]{1,0:T(8,128)S(1)}) fusion(f32[256,128]{1,0:T(8,128)S(1)} %copy.243, f32[256,128]{1,0:T(8,128)S(1)} %dynamic-slice_bitcast_fusion.8, f32[256,128]{1,0:T(8,128)} %copy.244, pred[128,128]{1,0:T(8,128)(4,1)S(1)} %iota_compare_fusion.3), kind=kLoop, calls=%fused_computation.19.clone.1 | loop fusion | flops 29294592 | bytes 671744 | tf_op jit(solution)/shard_map/transpose(jvp())/while/body/eval_jaxpr/checkpoint/reduce_sum | solution.py:34
  208.0 2.2 reduce_window_sum.48
  211.9 1.3 constant_dynamic-slice_fusion.7
  214.9 15.3 %fusion.104 = f32[256,1,128]{2,1,0:T(1,128)S(1)} fusion(f32[256,128,1]{1,2,0:T(1,128)S(1)} %copy.247, f32[256,128]{1,0:T(8,128)S(1)} %copy.243, pred[128,128]{1,0:T(8,128)(4,1)S(1)} %iota_compare_fusion.3), kind=kOutput, calls=%fused_computation.17.clone.1 | convolution fusion | flops 58720256 | bytes 409600 | tf_op jit(solution)/shard_map/transpose(jvp())/while/body/eval_jaxpr/checkpoint/cts,cs->ct/dot_general | solution.py:36
  231.6 16.3 %fusion.103 = (f32[256,128]{1,0:T(8,128)}, f32[256,128]{1,0:T(8,128)S(1)}) fusion(f32[256,128]{1,0:T(8,128)S(1)} %copy.243, f32[256,128]{1,0:T(8,128)S(1)} %dynamic-slice_bitcast_fusion.8, f32[256,128]{1,0:T(8,128)} %copy.244, pred[128,128]{1,0:T(8,128)(4,1)S(1)} %iota_compare_fusion.3), kind=kLoop, calls=%fused_computation.19.clone.1 | loop fusion | flops 29294592 | bytes 671744 | tf_op jit(solution)/shard_map/transpose(jvp())/while/body/eval_jaxpr/checkpoint/reduce_sum | solution.py:34
  249.7 2.2 reduce_window_sum.48
  253.7 1.3 constant_dynamic-slice_fusion.7
  256.6 15.3 %fusion.104 = f32[256,1,128]{2,1,0:T(1,128)S(1)} fusion(f32[256,128,1]{1,2,0:T(1,128)S(1)} %copy.247, f32[256,128]{1,0:T(8,128)S(1)} %copy.243, pred[128,128]{1,0:T(8,128)(4,1)S(1)} %iota_compare_fusion.3), kind=kOutput, calls=%fused_computation.17.clone.1 | convolution fusion | flops 58720256 | bytes 409600 | tf_op jit(solution)/shard_map/transpose(jvp())/while/body/eval_jaxpr/checkpoint/cts,cs->ct/dot_general | solution.py:36
  273.4 16.3 %fusion.103 = (f32[256,128]{1,0:T(8,128)}, f32[256,128]{1,0:T(8,128)S(1)}) fusion(f32[256,128]{1,0:T(8,128)S(1)} %copy.243, f32[256,128]{1,0:T(8,128)S(1)} %dynamic-slice_bitcast_fusion.8, f32[256,128]{1,0:T(8,128)} %copy.244, pred[128,128]{1,0:T(8,128)(4,1)S(1)} %iota_compare_fusion.3), kind=kLoop, calls=%fused_computation.19.clone.1 | loop fusion | flops 29294592 | bytes 671744 | tf_op jit(solution)/shard_map/transpose(jvp())/while/body/eval_jaxpr/checkpoint/reduce_sum | solution.py:34
  291.5 2.2 reduce_window_sum.48
  295.5 1.3 constant_dynamic-slice_fusion.7
  298.4 15.3 %fusion.104 = f32[256,1,128]{2,1,0:T(1,128)S(1)} fusion(f32[256,128,1]{1,2,0:T(1,128)S(1)} %copy.247, f32[256,128]{1,0:T(8,128)S(1)} %copy.243, pred[128,128]{1,0:T(8,128)(4,1)S(1)} %iota_compare_fusion.3), kind=kOutput, calls=%fused_computation.17.clone.1 | convolution fusion | flops 58720256 | bytes 409600 | tf_op jit(solution)/shard_map/transpose(jvp())/while/body/eval_jaxpr/checkpoint/cts,cs->ct/dot_general | solution.py:36
  315.1 16.3 %fusion.103 = (f32[256,128]{1,0:T(8,128)}, f32[256,128]{1,0:T(8,128)S(1)}) fusion(f32[256,128]{1,0:T(8,128)S(1)} %copy.243, f32[256,128]{1,0:T(8,128)S(1)} %dynamic-slice_bitcast_fusion.8, f32[256,128]{1,0:T(8,128)} %copy.244, pred[128,128]{1,0:T(8,128)(4,1)S(1)} %iota_compare_fusion.3), kind=kLoop, calls=%fused_computation.19.clone.1 | loop fusion | flops 29294592 | bytes 671744 | tf_op jit(solution)/shard_map/transpose(jvp())/while/body/eval_jaxpr/checkpoint/reduce_sum | solution.py:34
  333.3 2.2 reduce_window_sum.48
  336.4 1.3 copy.194
  338.2 2.3 fusion.52
  340.5 1.4 fusion.75
  341.9 1.4 copy.202
  344.4 1.3 fusion.45
  345.7 1.3 convolution_convert_fusion.2
  347.0 1.6 fusion.48
  351.3 2.2 reduce.3
  354.3 5.1 %all-to-all-start.1 = ((bf16[4,2,16384]{2,1,0:T(2,128)(2,1)}), bf16[4,2,16384]{2,1,0:T(2,128)(2,1)S(1)}, u32[]{:S(2)}, u32[]{:S(2)}) async-start(bf16[4,2,16384]{2,1,0:T(2,128)(2,1)} %reshape.213), calls=%async_computation.1 | async-start | bytes 524288 | tf_op jit(solution)/shard_map/all_to_all | solution.py:120
  362.0 5.6 %all-to-all-done.1 = bf16[4,2,16384]{2,1,0:T(2,128)(2,1)S(1)} async-done(((bf16[4,2,16384]{2,1,0:T(2,128)(2,1)}), bf16[4,2,16384]{2,1,0:T(2,128)(2,1)S(1)}, u32[]{:S(2)}, u32[]{:S(2)}) %all-to-all-start.1) | async-done | bytes 262176 | tf_op jit(solution)/shard_map/all_to_all | solution.py:120
  369.6 30.7 %all_to_all.29 = bf16[8,1,128,1024]{2,3,1,0:T(8,128)(2,1)S(1)} all-to-all(bf16[8,1,128,1024]{2,3,1,0:T(8,128)(2,1)S(1)} %fusion.60), channel_id=1, replica_groups=mesh['sp'=4,'dp'=8] {'dp'}, dimensions={0} | all-to-all | bytes 4194304 | tf_op jit(solution)/shard_map/all_to_all | solution.py:17
  403.2 15.5 %all-reduce.13.cloned.1.call-done = (bf16[4,256]{1,0:T(4,128)(2,1)}, bf16[4,64,64]{2,1,0:T(8,128)(2,1)}, bf16[4,64,64]{2,1,0:T(8,128)(2,1)}, bf16[256]{0:T(256)(128)(2,1)}) async-done(((bf16[4,256]{1,0:T(4,128)(2,1)}, bf16[4,64,64]{2,1,0:T(8,128)(2,1)}, bf16[4,64,64]{2,1,0:T(8,128)(2,1)}, bf16[256]{0:T(256)(128)(2,1)}), (bf16[4,256]{1,0:T(4,128)(2,1)}, bf16[4,64,64]{2,1,0:T(8,128)(2,1)}, ...) | async-done | bytes 68112 | tf_op jit(solution)/shard_map/psum | solution.py:114
  418.7 1.5 convert_element_type.122
  420.2 1.5 convert_element_type.124
  421.7 1.3 convert_element_type.120
  424.1 25.0 %all-gather.2.cloned.1.call-done = bf16[1024,1024]{1,0:T(8,128)(2,1)} async-done(((bf16[128,1024]{1,0:T(8,128)(2,1)}), bf16[1024,1024]{1,0:T(8,128)(2,1)}) %all-gather.2.cloned.1.call-update) | async-done | bytes 2097168 | tf_op jit(solution)/shard_map/all_gather | solution.py:122
  449.1 2.4 fusion.27
  (242 shorter events, 60.5 us)
Async XLA Ops:
  8.0 360.2 %copy-start = (bf16[1,1024,128]{2,1,0:T(8,128)(2,1)S(1)}, bf16[1,1024,128]{2,1,0:T(8,128)(2,1)}, u32[]{:S(2)}) copy-start(bf16[1,1024,128]{2,1,0:T(8,128)(2,1)} %param.14) | copy-start | bytes 786436
  8.0 11.4 %copy-start.39 = (f32[4,256]{1,0:T(4,128)S(1)}, f32[4,256]{1,0:T(4,128)}, u32[]{:S(2)}) copy-start(f32[4,256]{1,0:T(4,128)} %param.19) | copy-start | bytes 12292
  8.0 11.4 %copy-start.13 = (bf16[1,256,512]{2,1,0:T(8,128)(2,1)S(1)}, bf16[1,256,512]{2,1,0:T(8,128)(2,1)}, u32[]{:S(2)}) copy-start(bf16[1,256,512]{2,1,0:T(8,128)(2,1)} %param.15) | copy-start | bytes 786436
  8.0 12.1 %copy-start.19 = (f32[4,64,64]{2,1,0:T(8,128)S(1)}, f32[4,64,64]{2,1,0:T(8,128)}, u32[]{:S(2)}) copy-start(f32[4,64,64]{2,1,0:T(8,128)} %param.20) | copy-start | bytes 196612
  13.0 148.1 %all-to-all-start = ((bf16[4,2,16384]{2,1,0:T(2,128)(2,1)}), bf16[4,2,16384]{2,1,0:T(2,128)(2,1)}, u32[]{:S(2)}, u32[]{:S(2)}) async-start(bf16[4,2,16384]{2,1,0:T(2,128)(2,1)} %reshape.211), calls=%async_computation | async-start | bytes 524288 | tf_op jit(solution)/shard_map/all_to_all | solution.py:102
  19.3 1.6 copy-start.17
  19.4 2.8 copy-start.23
  19.4 2.8 copy-start.25
  19.4 2.8 copy-start.28
  19.4 2.8 copy-start.31
  20.2 1.5 copy-start.1
  20.2 1.4 copy-start.37
  20.2 2.0 copy-start.15
  22.2 136.2 %copy-start.21 = (f32[256]{0:T(256)}, f32[256]{0:T(256)S(1)}, u32[]{:S(2)}) copy-start(f32[256]{0:T(256)S(1)} %get-tuple-element.473) | copy-start | bytes 3076
  160.1 7.5 %copy-start.7 = (bf16[1,256,512]{1,2,0:T(8,128)(2,1)}, bf16[1,256,512]{1,2,0:T(8,128)(2,1)S(1)}, u32[]{:S(2)}) copy-start(bf16[1,256,512]{1,2,0:T(8,128)(2,1)S(1)} %copy.185) | copy-start | bytes 786436
  164.0 0.7 copy-start.5
  336.4 1.6 copy-start.10
  336.4 1.8 copy-start.16
  336.4 1.8 copy-start.22
  336.4 1.8 copy-start.24
  336.4 1.8 copy-start.26
  336.4 1.8 copy-start.29
  336.4 1.8 copy-start.32
  337.9 2.6 copy-start.3
  338.2 2.3 copy-start.18
  341.9 3.8 copy-start.2
  343.4 3.6 copy-start.20
  344.4 2.6 copy-start.11
  344.4 2.6 copy-start.12
  344.4 2.6 copy-start.14
  344.4 2.6 copy-start.35
  345.7 3.0 copy-start.4
  348.6 0.9 copy-start.36
  348.6 1.0 copy-start.34
  348.6 1.0 copy-start.38
  348.6 1.0 copy-start.40
  348.6 1.5 copy-start.27
  348.6 1.5 copy-start.30
  348.7 1.5 copy-start.33
  354.3 13.4 %all-to-all-start.1 = ((bf16[4,2,16384]{2,1,0:T(2,128)(2,1)}), bf16[4,2,16384]{2,1,0:T(2,128)(2,1)S(1)}, u32[]{:S(2)}, u32[]{:S(2)}) async-start(bf16[4,2,16384]{2,1,0:T(2,128)(2,1)} %reshape.213), calls=%async_computation.1 | async-start | bytes 524288 | tf_op jit(solution)/shard_map/all_to_all | solution.py:120
  359.4 59.3 %all-reduce.13.cloned.1.call-start = ((), (), s32[]{:S(2)}) async-start(), calls=%async_computation.6 | async-start | bytes 267264 | tf_op jit(solution)/shard_map/psum | solution.py:114
  361.2 87.9 %all-gather.2.cloned.1.call-start = ((), (), s32[]{:S(2)}) async-start(), calls=%async_computation.4 | async-start | bytes 2359296 | tf_op jit(solution)/shard_map/all_gather | solution.py:122
  362.0 90.4 %reduce-scatter.2.cloned.1.call-start = ((), (), s32[]{:S(2)}) async-start(), calls=%async_computation.5 | async-start | bytes 655360 | tf_op jit(solution)/shard_map/reduce_scatter | solution.py:141
  400.3 1.4 copy-start.6
  400.6 1.3 copy-start.8
  400.6 1.3 copy-start.9
Sparse Core Ops, SparseCore 0:
  364.2 54.3 all-reduce.12
  420.6 28.4 all-gather.1
Sparse Core Ops, SparseCore 1:
  401.7 19.3 reduce-scatter.1
